TPU v7x, 32 devices: a whole 2x2x4 slice. The times are simulated.
32 devices in a mesh: fs: 8 (over z, y), tp: 4 (over x, core).
Axes of the slice: x: 2, y: 2, z: 4, core: 2. Of those that a mesh axis runs over, the one named last changes fastest.
Arguments:
- tokens: bfloat16 [8192, 2048], P('fs'), may hold values from -6 to 6
- norm_gain: float32 [2048], P('fs'), may hold values from 0.1 to 1.9
- gate_train: float32 [8, 2048, 768], P(None, 'fs', 'tp'), may hold values from -0.125 to 0.125
- up_train: float32 [8, 2048, 768], P(None, 'fs', 'tp'), may hold values from -0.125 to 0.125
- down_train: float32 [8, 768, 2048], P(None, 'fs', 'tp'), may hold values from -0.21875 to 0.21875
- expert_ids: int32 [8192, 2], P('fs'), may hold values from 0 to 7, all different within a row; in each aligned block of 1024 rows (0 to 1023, 1024 to 2047, ...) at most 512 rows name the same one
- route_weights: float32 [8192, 2], P('fs'), may hold values from 0.1 to 1
Outputs:
- gate_serve: bfloat16 [8, 2048, 768], P('fs', None, 'tp')
- up_serve: bfloat16 [8, 2048, 768], P('fs', None, 'tp')
- down_serve: bfloat16 [8, 768, 2048], P('fs', 'tp')
- mixed: bfloat16 [8192, 2048], P('fs', 'tp')
Inputs may be any that keep to these rules, and one draw needn't show every extreme that they name: `expert_ids`: each row names 2 different experts. Within each aligned block of 1024 rows no expert is named more than 512 times, and in every block some expert is named exactly 512 times; every expert is named somewhere.
All inputs are finite; a program needn't handle non-finite values.
Results may differ from a plain program's by a relative error of at most 0.011.
Values may be sent and summed in bfloat16 or wider, within the bound.
A program may use at most 128 MiB of HBM per device.

v0:
```python
import jax
import jax.numpy as jnp
from jax import lax
from jax.sharding import PartitionSpec as P

epsilon = 1e-06


def on_device(tokens, norm_gain, gate_train, up_train, down_train, expert_ids, route_weights):
    experts, rows, cols = gate_train.shape
    fs_at = lax.axis_index("fs")
    tok_rows, picks = expert_ids.shape
    down_rows, down_cols = down_train.shape[1:]
    fs_count = lax.axis_size("fs")
    gate_up = jnp.concatenate(
        [norm_gain[None, :, None] * gate_train, norm_gain[None, :, None] * up_train], axis=2
    ).astype(jnp.bfloat16)
    gate_up = gate_up.transpose(1, 0, 2).reshape(rows, experts * 2 * cols)
    gate_up_all = lax.all_gather(gate_up, "fs", axis=0, tiled=True)
    down_all = lax.all_gather(
        down_train.astype(jnp.bfloat16).reshape(experts * down_rows, down_cols),
        "fs",
        axis=0,
        tiled=True,
    )
    tok_float = tokens.astype(jnp.float32)
    normed = (
        tok_float * lax.rsqrt(jnp.mean(tok_float * tok_float, axis=-1, keepdims=True) + epsilon)
    ).astype(jnp.bfloat16)
    shares = route_weights / jnp.sum(route_weights, axis=-1, keepdims=True)
    group = 2 * lax.axis_size("tp")
    picked = [jnp.zeros((tok_rows, cols), jnp.float32) for _ in range(picks)]
    for first in range(0, experts, group):
        part = gate_up_all[:, first * 2 * cols : (first + group) * 2 * cols]
        if first:
            part, picked = lax.optimization_barrier((part, picked))
        acts = jnp.dot(normed, part, preferred_element_type=jnp.float32)
        for at in range(group):
            g = acts[:, at * 2 * cols : at * 2 * cols + cols]
            u = acts[:, at * 2 * cols + cols : (at + 1) * 2 * cols]
            h = jax.nn.silu(g) * u
            for k in range(picks):
                picked[k] = picked[k] + jnp.where(expert_ids[:, k : k + 1] == first + at, h, 0.0)
    hidden = jnp.stack([picked[k] * shares[:, k : k + 1] for k in range(picks)], 0)
    hidden_all = lax.all_gather(hidden.astype(jnp.bfloat16), "tp", axis=2, tiled=True)
    hidden_all = hidden_all.reshape(picks, tok_rows, fs_count, 1, down_rows)
    ids = jnp.arange(experts, dtype=jnp.int32)[None, None, :, None]
    mixed = jnp.zeros((tok_rows, down_cols), jnp.float32)
    for first in range(0, fs_count, group):
        blocks = hidden_all[:, :, first : first + group]
        if first:
            blocks, mixed = lax.optimization_barrier((blocks, mixed))
        spread = jnp.zeros((tok_rows, group, experts, down_rows), jnp.bfloat16)
        for k in range(picks):
            spread = jnp.where(expert_ids[:, k][:, None, None, None] == ids, blocks[k], spread)
        depth = experts * down_rows
        mixed = mixed + jnp.dot(
            spread.reshape(tok_rows, group * depth),
            down_all[first * depth : (first + group) * depth],
            preferred_element_type=jnp.float32,
        )
    mixed = mixed.astype(jnp.bfloat16)
    own = lax.dynamic_slice_in_dim(gate_up_all, fs_at * 2 * cols, 2 * cols, 1)
    down_own = lax.dynamic_slice_in_dim(
        down_all.reshape(fs_count, experts, down_rows, down_cols), fs_at, 1, 1
    ).reshape(1, fs_count * down_rows, down_cols)
    down_serve = lax.all_to_all(down_own, "tp", split_axis=1, concat_axis=2, tiled=True)
    return (own[None, :, :cols], own[None, :, cols:], down_serve, mixed)


def solution(mesh):
    return jax.shard_map(
        on_device,
        mesh=mesh,
        in_specs=(
            P("fs", None),
            P("fs"),
            P(None, "fs", "tp"),
            P(None, "fs", "tp"),
            P(None, "fs", "tp"),
            P("fs", None),
            P("fs", None),
        ),
        out_specs=(P("fs", None, "tp"), P("fs", None, "tp"), P("fs", "tp", None), P("fs", "tp")),
        check_vma=False,
    )
```

profile of v0, /device:TPU:0, one launch (start us, length us, event | category | flops | bytes accessed | tf_op | source)
XLA Modules:
  0.0 353.5 jit_solution(751838854216082823)
XLA Ops:
  7.2 0.0 copy-start
  7.2 0.0 all-gather.4.cloned.1.call-start
  7.2 2.3 multiply_convert_fusion.1
  9.6 0.0 copy-start.2
  9.6 0.0 copy-start.1
  9.6 1.3 pad_maximum_fusion
  10.9 0.0 all-gather.4.cloned.1.call-update
  10.9 0.0 all-gather.6.cloned.1.call-start
  10.9 0.0 copy-done
  10.9 1.0 convert_element_type.14
  11.9 0.0 all-gather.6.cloned.1.call-update
  11.9 0.0 all-gather.8.cloned.1.call-start
  12.0 0.0 copy-done.2
  12.0 0.0 copy-done.1
  12.0 0.2 compare_reduce_fusion.15
  12.2 3.1 fusion
  15.4 174.5 %all-gather.4.cloned.1.call-done = bf16[2048,3072]{0,1:T(8,128)(2,1)} async-done(((bf16[256,3072]{0,1:T(8,128)(2,1)}), bf16[2048,3072]{0,1:T(8,128)(2,1)}) %all-gather.4.cloned.1.call-update) | async-done | bytes 12582928 | tf_op jit(solution)/shard_map/all_gather | solution.py:19
  189.9 17.1 %fusion.2 = f32[1024,3072]{1,0:T(8,128)S(1)} fusion(bf16[2048,3072]{0,1:T(8,128)(2,1)} %all-gather.4.cloned.1.call-done, bf16[1024,2048]{1,0:T(8,128)(2,1)} %param.7, f32[1024]{0:T(1024)S(1)} %add_rsqrt_fusion), kind=kOutput, calls=%fused_computation.5 | convolution fusion | flops 12891193344 | bytes 29364224 | tf_op jit(solution)/shard_map/dot_general | solution.py:37
  207.0 4.5 %fusion.5 = bf16[1,1024,192]{2,1,0:T(8,128)(2,1)S(1)} fusion(f32[1024]{0:T(1024)S(1)} %bitcast.47, pred[1024]{0:T(1024)(128)(4,1)S(1)} %get-tuple-element.19, pred[1024]{0:T(1024)(128)(4,1)S(1)} %get-tuple-element.18, pred[1024]{0:T(1024)(128)(4,1)S(1)} %get-tuple-element.17, pred[1024]{0:T(1024)(128)(4,1)S(1)} %get-tuple-element.16, ...), kind=kLoop, calls=%fused_computation.24 | loop fusion | flops 11206656 | bytes 12988416 | tf_op jit(solution)/shard_map/stack | solution.py:44
  211.5 4.5 %fusion.6 = bf16[1,1024,192]{2,1,0:T(8,128)(2,1)S(1)} fusion(f32[1024]{0:T(1024)S(1)} %bitcast.46, pred[1024]{0:T(1024)(128)(4,1)S(1)} %get-tuple-element.12, pred[1024]{0:T(1024)(128)(4,1)S(1)} %get-tuple-element.11, pred[1024]{0:T(1024)(128)(4,1)S(1)} %get-tuple-element.10, pred[1024]{0:T(1024)(128)(4,1)S(1)} %get-tuple-element.9, ...), kind=kLoop, calls=%fused_computation.25 | loop fusion | flops 11206656 | bytes 12988416 | tf_op jit(solution)/shard_map/stack | solution.py:44
  216.0 0.2 pad_maximum_fusion.1
  216.2 2.0 copy.22
  218.2 0.0 all-gather.8.cloned.1.call-update
  218.2 71.3 %all-gather.6.cloned.1.call-done = bf16[6144,512]{1,0:T(8,128)(2,1)} async-done(((bf16[768,512]{1,0:T(8,128)(2,1)}), bf16[6144,512]{1,0:T(8,128)(2,1)}) %all-gather.6.cloned.1.call-update) | async-done | bytes 6291472 | tf_op jit(solution)/shard_map/all_gather | solution.py:20
  289.5 1.2 constant_dynamic-slice_fusion
  290.8 1.2 copy.30
  292.0 0.5 broadcast.126
  292.5 5.4 %reduce.32 = bf16[768,512]{1,0:T(8,128)(2,1)S(1)} reduce(bf16[768,1,512]{2,1,0:T(2,128)(2,1)S(1)} %bitcast.37, bf16[]{:T(256)} %broadcast.126), dimensions={1}, to_apply=%bitcast.32.reduce_sub_computation | reduce | bytes 1572866
  297.9 1.4 reshape.117
  299.3 3.7 %all-to-all-start = ((bf16[4,2,49152]{2,1,0:T(2,128)(2,1)}), bf16[4,2,49152]{2,1,0:T(2,128)(2,1)S(1)}, u32[]{:S(2)}, u32[]{:S(2)}) async-start(bf16[4,2,49152]{2,1,0:T(2,128)(2,1)} %reshape.117), calls=%async_computation | async-start | bytes 1572864 | tf_op jit(solution)/shard_map/all_to_all | solution.py:67
  303.0 20.2 %all-to-all-done = bf16[4,2,49152]{2,1,0:T(2,128)(2,1)S(1)} async-done(((bf16[4,2,49152]{2,1,0:T(2,128)(2,1)}), bf16[4,2,49152]{2,1,0:T(2,128)(2,1)S(1)}, u32[]{:S(2)}, u32[]{:S(2)}) %all-to-all-start) | async-done | bytes 786464 | tf_op jit(solution)/shard_map/all_to_all | solution.py:67
  323.2 0.7 reshape.118
  324.0 0.2 copy.25
  324.2 1.0 copy.28
  325.2 2.7 dynamic-slice_bitcast_fusion
  327.9 0.0 all-gather.8.cloned.1.call-done
  327.9 7.8 %fusion.7 = (bf16[1,1024,768]{1,0,2:T(2,128)(2,1)S(1)}, bf16[1,1024,768]{1,0,2:T(2,128)(2,1)S(1)}) fusion(bf16[2,1024,768]{1,0,2:T(2,128)(2,1)} %all-gather.8.cloned.1.call-done), kind=kLoop, calls=%fused_computation.47 | loop fusion | bytes 6291456 | tf_op jit(solution)/shard_map/slice | solution.py:55
  335.7 0.6 copy.26
  336.3 0.0 slice-start
  336.3 0.6 copy.27
  336.9 0.0 slice-start.1
  336.9 1.9 select_select_fusion
  338.8 0.0 slice-done
  338.8 0.5 slice-done.1
  339.3 7.6 %convolution_convert_fusion = bf16[1024,512]{1,0:T(8,128)(2,1)} fusion(bf16[1024,6144]{0,1:T(8,128)(2,1)S(1)} %bitcast.33, bf16[6144,512]{1,0:T(8,128)(2,1)S(1)} %bitcast.45), kind=kOutput, calls=%fused_computation.10 | convolution fusion | flops 6442975232 | bytes 19922944 | tf_op jit(solution)/shard_map/dot_general | solution.py:57
  (7 shorter events, 0.1 us)
Async XLA Ops:
  7.2 3.8 %copy-start = (f32[8,96,512]{2,1,0:T(8,128)S(1)}, f32[8,96,512]{2,1,0:T(8,128)}, u32[]{:S(2)}) copy-start(f32[8,96,512]{2,1,0:T(8,128)} %param.11) | copy-start | bytes 4718596
  7.2 182.7 %all-gather.4.cloned.1.call-start = ((), (), s32[]{:S(2)}) async-start(), calls=%async_computation.1 | async-start | bytes 14155776 | tf_op jit(solution)/shard_map/all_gather | solution.py:19
  9.6 2.4 copy-start.2
  9.6 2.5 copy-start.1
  10.9 278.7 %all-gather.6.cloned.1.call-start = ((), (), s32[]{:S(2)}) async-start(), calls=%async_computation.2 | async-start | bytes 7077888 | tf_op jit(solution)/shard_map/all_gather | solution.py:20
  11.9 315.9 %all-gather.8.cloned.1.call-start = ((), (), s32[]{:S(2)}) async-start(), calls=%async_computation.3 | async-start | bytes 3932160 | tf_op jit(solution)/shard_map/all_gather | solution.py:45
  299.3 23.9 %all-to-all-start = ((bf16[4,2,49152]{2,1,0:T(2,128)(2,1)}), bf16[4,2,49152]{2,1,0:T(2,128)(2,1)S(1)}, u32[]{:S(2)}, u32[]{:S(2)}) async-start(bf16[4,2,49152]{2,1,0:T(2,128)(2,1)} %reshape.117), calls=%async_computation | async-start | bytes 1572864 | tf_op jit(solution)/shard_map/all_to_all | solution.py:67
  336.3 2.5 slice-start
  336.9 2.4 slice-start.1
Sparse Core Ops, SparseCore 0:
  11.0 178.8 all-gather.3
  192.6 96.8 all-gather.5
  291.7 35.1 all-gather.7
where the time goes:
time: 354 us; the launch traced here: 353 us
  waiting for transfers between devices  266 us (75%)
  matrix products  24.7 us (7%)
  other arithmetic  24.4 us (7%)
  local copies, waits for them, and re-layouts  20.5 us (6%)
  between operations  14 us (4%)
  starting transfers between devices  3.8 us (1%)
    all_gather x1, waiting for transfers between devices, on_device(): gate_up_all = lax.all_gather(gate_up, 'fs', axis=0, tiled=True)  175 us
    all_gather x1, waiting for transfers between devices, on_device(): lax.all_gather(down_train.astype(jnp.bfloat16).reshape(experts * down_row...  71.3 us
    all_to_all x1, waiting for transfers between devices, on_device(): lax.all_to_all(down_own, 'tp', split_axis=1, concat_axis=2, tiled=True)  20.2 us
    dot_general x1, matrix products, on_device(): acts = jnp.dot(normed, part, preferred_element_type=jnp.float32)  17.1 us
    another operation x3, other arithmetic, on_device(): jnp.stack([picked[k] * shares[:, k:k + 1] for k in range(picks)], 0)  9.18 us
    slice x1, local copies, waits for them, and re-layouts, on_device(): blocks[k]  7.82 us
    dot_general x1, matrix products, on_device(): jnp.dot(spread.reshape(tok_rows, group * depth), down_all[first * depth:(...  7.64 us
  transfers between devices with their start and end apart: 4, of which 3 were waited for; matrix products, arithmetic and copies ran while one was open for 13% of the time, Pallas kernels for 0%

commit v1 on v0

--- a/solution.py
+++ b/solution.py
@@ -6,7 +6,26 @@
 epsilon = 1e-06
 
 
+def load_the_spot(mine, dim_i):
+    b_next = list(mine.shape[1:])
+    b_next[dim_i] *= mine.shape[0]
+    return jnp.moveaxis(mine, 0, dim_i).reshape(b_next)
+
+
 def on_device(tokens, norm_gain, gate_train, up_train, down_train, expert_ids, route_weights):
+
+    def solve_the_thing(v0, peer_axis, axis_no):
+        n_axis = lax.psum(1, peer_axis)
+        all_blocks = [(ix, (ix + 1) % n_axis) for ix in range(n_axis)]
+        inbox = [v0]
+        while len(inbox) < n_axis:
+            last = lax.ppermute(inbox[-1], peer_axis, all_blocks)
+            inbox.append(last)
+        left_arr = lax.axis_index(peer_axis)
+        block_out = jnp.stack(inbox, 0)
+        inbox = block_out[(left_arr - jnp.arange(n_axis)) % n_axis]
+        return load_the_spot(inbox, axis_no)
+
     experts, rows, cols = gate_train.shape
     fs_at = lax.axis_index("fs")
     tok_rows, picks = expert_ids.shape
@@ -16,7 +35,7 @@
         [norm_gain[None, :, None] * gate_train, norm_gain[None, :, None] * up_train], axis=2
     ).astype(jnp.bfloat16)
     gate_up = gate_up.transpose(1, 0, 2).reshape(rows, experts * 2 * cols)
-    gate_up_all = lax.all_gather(gate_up, "fs", axis=0, tiled=True)
+    gate_up_all = solve_the_thing(gate_up, "fs", 0)
     down_all = lax.all_gather(
         down_train.astype(jnp.bfloat16).reshape(experts * down_rows, down_cols),
         "fs",

time: 354 us -> 445 us (1.26)
  waiting for transfers between devices: 266 us -> 322 us
  local copies, waits for them, and re-layouts: 20.5 us -> 53.7 us
    ppermute x0 -> x7, waiting for transfers between devices: none -> 309 us  [solve_the_thing(): last = lax.ppermute(inbox[-1], peer_axis, all_blocks)]
    all_gather x1 -> x0, waiting for transfers between devices: 175 us -> none  [on_device(): gate_up_all = lax.all_gather(gate_up, 'fs', axis=0, tiled=True)]
    all_gather x1, waiting for transfers between devices: 71.3 us -> 0.02 us  [on_device(): lax.all_gather(down_train.astype(jnp.bfloat16).reshape(experts * down_row...]
    unnamed x16 -> x33, local copies, waits for them, and re-layouts: 4.54 us -> 22.7 us
    gather x0 -> x1, local copies, waits for them, and re-layouts: none -> 11.1 us  [solve_the_thing(): inbox = block_out[(left_arr - jnp.arange(n_axis)) % n_axis]]
    all_to_all x1, waiting for transfers between devices: 20.2 us -> 13.2 us  [on_device(): lax.all_to_all(down_own, 'tp', split_axis=1, concat_axis=2, tiled=True)]
  transfers between devices with their start and end apart: 4 -> 10, of which waited for: 3 -> 8; matrix products, arithmetic and copies ran while one was open for 13% -> 17% of each run, Pallas kernels for 0% -> 0%
where the time goes in v1:
time: 445 us
  waiting for transfers between devices  322 us (72%)
  local copies, waits for them, and re-layouts  53.7 us (12%)
  matrix products  24.8 us (6%)
  other arithmetic  23.5 us (5%)
  between operations  14.3 us (3%)
  starting transfers between devices  6.61 us (1%)
    ppermute x7, waiting for transfers between devices, solve_the_thing(): last = lax.ppermute(inbox[-1], peer_axis, all_blocks)  309 us
    unnamed x33, local copies, waits for them, and re-layouts  22.7 us
    dot_general x1, matrix products, on_device(): acts = jnp.dot(normed, part, preferred_element_type=jnp.float32)  17.1 us
    all_to_all x1, waiting for transfers between devices, on_device(): lax.all_to_all(down_own, 'tp', split_axis=1, concat_axis=2, tiled=True)  13.2 us
    gather x1, local copies, waits for them, and re-layouts, solve_the_thing(): inbox = block_out[(left_arr - jnp.arange(n_axis)) % n_axis]  11.1 us
    another operation x3, other arithmetic, on_device(): jnp.stack([picked[k] * shares[:, k:k + 1] for k in range(picks)], 0)  9.27 us
  transfers between devices with their start and end apart: 10, of which 8 were waited for; matrix products, arithmetic and copies ran while one was open for 17% of the time, Pallas kernels for 0%

profile of v1, /device:TPU:0, one launch (start us, length us, event | category | flops | bytes accessed | tf_op | source)
XLA Modules:
  0.0 444.7 jit_solution(10951594704178108077)
XLA Ops:
  7.2 2.3 multiply_convert_fusion.1
  9.7 1.8 copy.38
  11.5 3.0 collective-permute-start
  14.5 37.6 %collective-permute-done = bf16[256,3072]{1,0:T(8,128)(2,1)S(1)} collective-permute-done((bf16[256,3072]{1,0:T(8,128)(2,1)}, bf16[256,3072]{1,0:T(8,128)(2,1)S(1)}, u32[]{:S(2)}, u32[]{:S(2)}) %collective-permute-start) | collective-permute-done | bytes 1572896 | tf_op jit(solution)/shard_map/ppermute | solution.py:22
  52.1 1.2 copy-done.1
  53.3 38.3 %collective-permute-done.1 = bf16[256,3072]{1,0:T(8,128)(2,1)S(1)} collective-permute-done((bf16[256,3072]{1,0:T(8,128)(2,1)S(1)}, bf16[256,3072]{1,0:T(8,128)(2,1)S(1)}, u32[]{:S(2)}, u32[]{:S(2)}) %collective-permute-start.1) | collective-permute-done | bytes 1572896 | tf_op jit(solution)/shard_map/ppermute | solution.py:22
  91.5 1.2 copy-done.3
  92.7 37.5 %collective-permute-done.2 = bf16[256,3072]{1,0:T(8,128)(2,1)} collective-permute-done((bf16[256,3072]{1,0:T(8,128)(2,1)S(1)}, bf16[256,3072]{1,0:T(8,128)(2,1)}, u32[]{:S(2)}, u32[]{:S(2)}) %collective-permute-start.2) | collective-permute-done | bytes 1572896 | tf_op jit(solution)/shard_map/ppermute | solution.py:22
  130.2 1.0 convert_element_type.14
  131.3 61.2 %collective-permute-done.3 = bf16[256,3072]{1,0:T(8,128)(2,1)} collective-permute-done((bf16[256,3072]{1,0:T(8,128)(2,1)}, bf16[256,3072]{1,0:T(8,128)(2,1)}, u32[]{:S(2)}, u32[]{:S(2)}) %collective-permute-start.3) | collective-permute-done | bytes 1572896 | tf_op jit(solution)/shard_map/ppermute | solution.py:22
  192.5 0.9 copy.37
  193.7 3.2 fusion
  196.9 1.3 constant_dynamic-update-slice_fusion
  198.2 63.2 %collective-permute-done.4 = bf16[256,3072]{1,0:T(8,128)(2,1)} collective-permute-done((bf16[256,3072]{1,0:T(8,128)(2,1)}, bf16[256,3072]{1,0:T(8,128)(2,1)}, u32[]{:S(2)}, u32[]{:S(2)}) %collective-permute-start.4) | collective-permute-done | bytes 1572896 | tf_op jit(solution)/shard_map/ppermute | solution.py:22
  261.3 1.2 bitcast_dynamic-update-slice_fusion.6
  262.6 1.2 bitcast_dynamic-update-slice_fusion.5
  263.8 2.7 bitcast_dynamic-update-slice_fusion.4
  266.5 45.3 %collective-permute-done.5 = bf16[256,3072]{1,0:T(8,128)(2,1)S(1)} collective-permute-done((bf16[256,3072]{1,0:T(8,128)(2,1)}, bf16[256,3072]{1,0:T(8,128)(2,1)S(1)}, u32[]{:S(2)}, u32[]{:S(2)}) %collective-permute-start.5) | collective-permute-done | bytes 1572896 | tf_op jit(solution)/shard_map/ppermute | solution.py:22
  311.8 2.7 bitcast_dynamic-update-slice_fusion.3
  314.5 2.7 bitcast_dynamic-update-slice_fusion.2
  317.2 1.3 bitcast_dynamic-update-slice_fusion.1
  318.5 25.5 %collective-permute-done.6 = bf16[256,3072]{1,0:T(8,128)(2,1)S(1)} collective-permute-done((bf16[256,3072]{1,0:T(8,128)(2,1)S(1)}, bf16[256,3072]{1,0:T(8,128)(2,1)S(1)}, u32[]{:S(2)}, u32[]{:S(2)}) %collective-permute-start.6) | collective-permute-done | bytes 1572896 | tf_op jit(solution)/shard_map/ppermute | solution.py:22
  344.0 1.2 bitcast_dynamic-update-slice_fusion
  345.2 11.1 %gather_fusion = bf16[8,256,3072]{2,1,0:T(8,128)(2,1)} fusion(bf16[8,256,3072]{2,1,0:T(8,128)(2,1)} %bitcast_dynamic-update-slice_fusion, s32[1024]{0:T(1024)S(1)} %pad_clamp_fusion), kind=kCustom, calls=%fused_computation | custom fusion | bytes 25165856 | tf_op jit(solution)/shard_map/gather | solution.py:26
  356.3 17.1 %fusion.2 = f32[1024,3072]{1,0:T(8,128)S(1)} fusion(bf16[2048,3072]{1,0:T(8,128)(2,1)} %bitcast.50, bf16[1024,2048]{1,0:T(8,128)(2,1)} %param.7, f32[1024]{0:T(1024)S(1)} %add_rsqrt_fusion), kind=kOutput, calls=%fused_computation.6 | convolution fusion | flops 12891193344 | bytes 29364224 | tf_op jit(solution)/shard_map/dot_general | solution.py:56
  373.4 4.5 %fusion.5 = bf16[1,1024,192]{2,1,0:T(8,128)(2,1)S(1)} fusion(f32[1024]{0:T(1024)S(1)} %bitcast.69, pred[1024]{0:T(1024)(128)(4,1)S(1)} %get-tuple-element.19, pred[1024]{0:T(1024)(128)(4,1)S(1)} %get-tuple-element.18, pred[1024]{0:T(1024)(128)(4,1)S(1)} %get-tuple-element.17, pred[1024]{0:T(1024)(128)(4,1)S(1)} %get-tuple-element.16, ...), kind=kLoop, calls=%fused_computation.30 | loop fusion | flops 11206656 | bytes 12988416 | tf_op jit(solution)/shard_map/stack | solution.py:63
  378.0 4.5 %fusion.6 = bf16[1,1024,192]{2,1,0:T(8,128)(2,1)S(1)} fusion(f32[1024]{0:T(1024)S(1)} %bitcast.68, pred[1024]{0:T(1024)(128)(4,1)S(1)} %get-tuple-element.12, pred[1024]{0:T(1024)(128)(4,1)S(1)} %get-tuple-element.11, pred[1024]{0:T(1024)(128)(4,1)S(1)} %get-tuple-element.10, pred[1024]{0:T(1024)(128)(4,1)S(1)} %get-tuple-element.9, ...), kind=kLoop, calls=%fused_computation.31 | loop fusion | flops 11206656 | bytes 12988416 | tf_op jit(solution)/shard_map/stack | solution.py:63
  382.5 0.2 pad_maximum_fusion.1
  382.7 2.0 copy.34
  384.8 1.2 constant_dynamic-slice_fusion.1
  386.1 1.2 copy.47
  387.3 0.5 broadcast.195
  387.8 5.4 %reduce.32 = bf16[768,512]{1,0:T(8,128)(2,1)S(1)} reduce(bf16[768,1,512]{2,1,0:T(2,128)(2,1)S(1)} %bitcast.57, bf16[]{:T(256)} %broadcast.195), dimensions={1}, to_apply=%bitcast.49.reduce_sub_computation | reduce | bytes 1572866
  393.2 1.6 reshape.178
  394.8 3.5 all-to-all-start
  398.4 3.0 constant_dynamic-slice_fusion.2
  401.4 1.2 copy.41
  402.6 1.2 copy.42
  403.9 13.2 %all-to-all-done = bf16[4,2,49152]{2,1,0:T(2,128)(2,1)S(1)} async-done(((bf16[4,2,49152]{2,1,0:T(2,128)(2,1)}), bf16[4,2,49152]{2,1,0:T(2,128)(2,1)S(1)}, u32[]{:S(2)}, u32[]{:S(2)}) %all-to-all-start) | async-done | bytes 786464 | tf_op jit(solution)/shard_map/all_to_all | solution.py:86
  417.1 0.7 reshape.179
  417.8 0.2 copy.39
  418.0 1.0 copy.45
  419.0 7.6 %fusion.9 = (bf16[1,1024,768]{1,0,2:T(2,128)(2,1)S(1)}, bf16[1,1024,768]{1,0,2:T(2,128)(2,1)S(1)}) fusion(bf16[2,1024,768]{1,0,2:T(2,128)(2,1)} %all-gather.5.cloned.1.call-done), kind=kLoop, calls=%fused_computation.63 | loop fusion | bytes 6291456 | tf_op jit(solution)/shard_map/slice | solution.py:74
  426.6 0.6 copy.43
  427.2 0.6 copy.44
  427.8 1.9 select_select_fusion
  429.7 0.5 slice-done.1
  430.2 7.6 %convolution_convert_fusion = bf16[1024,512]{1,0:T(8,128)(2,1)} fusion(bf16[1024,6144]{0,1:T(8,128)(2,1)S(1)} %bitcast.54, bf16[6144,512]{1,0:T(8,128)(2,1)S(1)} %bitcast.67), kind=kOutput, calls=%fused_computation.18 | convolution fusion | flops 6442975232 | bytes 19922944 | tf_op jit(solution)/shard_map/dot_general | solution.py:76
  (38 shorter events, 0.6 us)
Async XLA Ops:
  7.2 123.0 %copy-start = (f32[8,96,512]{2,1,0:T(8,128)S(1)}, f32[8,96,512]{2,1,0:T(8,128)}, u32[]{:S(2)}) copy-start(f32[8,96,512]{2,1,0:T(8,128)} %param.11) | copy-start | bytes 4718596
  7.2 377.6 %all-gather.3.cloned.1.call-start = ((), (), s32[]{:S(2)}) async-start(), calls=%async_computation.1 | async-start | bytes 7077888 | tf_op jit(solution)/shard_map/all_gather | solution.py:39
  9.6 183.8 %copy-start.6 = (f32[1024,2]{0,1:T(2,128)S(1)}, f32[1024,2]{0,1:T(2,128)}, u32[]{:S(2)}) copy-start(f32[1024,2]{0,1:T(2,128)} %param.13) | copy-start | bytes 24580
  9.6 183.9 %copy-start.5 = (s32[1024,2]{0,1:T(2,128)S(1)}, s32[1024,2]{0,1:T(2,128)}, u32[]{:S(2)}) copy-start(s32[1024,2]{0,1:T(2,128)} %param.12) | copy-start | bytes 24580
  11.5 40.6 %collective-permute-start = (bf16[256,3072]{1,0:T(8,128)(2,1)}, bf16[256,3072]{1,0:T(8,128)(2,1)S(1)}, u32[]{:S(2)}, u32[]{:S(2)}) collective-permute-start(bf16[256,3072]{1,0:T(8,128)(2,1)} %copy.38), channel_id=1, source_target_pairs={{0,4},{4,8},{8,12},{12,16},{16,20},{20,24},{24,28},{28,0},{1,5},{5... | collective-permute-start | bytes 4718600 | tf_op jit(solution)/shard_map/ppermute | solution.py:22
  52.1 1.2 copy-start.1
  53.3 38.3 %collective-permute-start.1 = (bf16[256,3072]{1,0:T(8,128)(2,1)S(1)}, bf16[256,3072]{1,0:T(8,128)(2,1)S(1)}, u32[]{:S(2)}, u32[]{:S(2)}) collective-permute-start(bf16[256,3072]{1,0:T(8,128)(2,1)S(1)} %collective-permute-done), channel_id=1, source_target_pairs={{0,4},{4,8},{8,12},{12,16},{16,20},{20,24},{24,28},{28,0},{1,5},{5... | collective-permute-start | bytes 4718600 | tf_op jit(solution)/shard_map/ppermute | solution.py:22
  91.5 1.2 copy-start.3
  92.7 37.5 %collective-permute-start.2 = (bf16[256,3072]{1,0:T(8,128)(2,1)S(1)}, bf16[256,3072]{1,0:T(8,128)(2,1)}, u32[]{:S(2)}, u32[]{:S(2)}) collective-permute-start(bf16[256,3072]{1,0:T(8,128)(2,1)S(1)} %collective-permute-done.1), channel_id=1, source_target_pairs={{0,4},{4,8},{8,12},{12,16},{16,20},{20,24},{24,28},{28,0},{1,5},{5... | collective-permute-start | bytes 4718600 | tf_op jit(solution)/shard_map/ppermute | solution.py:22
  130.2 62.3 %collective-permute-start.3 = (bf16[256,3072]{1,0:T(8,128)(2,1)}, bf16[256,3072]{1,0:T(8,128)(2,1)}, u32[]{:S(2)}, u32[]{:S(2)}) collective-permute-start(bf16[256,3072]{1,0:T(8,128)(2,1)} %collective-permute-done.2), channel_id=1, source_target_pairs={{0,4},{4,8},{8,12},{12,16},{16,20},{20,24},{24,28},{28,0},{1,5},{5... | collective-permute-start | bytes 4718600 | tf_op jit(solution)/shard_map/ppermute | solution.py:22
  131.2 287.8 %all-gather.5.cloned.1.call-start = ((), (), s32[]{:S(2)}) async-start(), calls=%async_computation.2 | async-start | bytes 3932160 | tf_op jit(solution)/shard_map/all_gather | solution.py:64
  192.5 68.8 %collective-permute-start.4 = (bf16[256,3072]{1,0:T(8,128)(2,1)}, bf16[256,3072]{1,0:T(8,128)(2,1)}, u32[]{:S(2)}, u32[]{:S(2)}) collective-permute-start(bf16[256,3072]{1,0:T(8,128)(2,1)} %collective-permute-done.3), channel_id=1, source_target_pairs={{0,4},{4,8},{8,12},{12,16},{16,20},{20,24},{24,28},{28,0},{1,5},{5... | collective-permute-start | bytes 4718600 | tf_op jit(solution)/shard_map/ppermute | solution.py:22
  193.4 67.9 %copy-start.2 = (bf16[256,3072]{1,0:T(8,128)(2,1)S(1)}, bf16[256,3072]{1,0:T(8,128)(2,1)}, u32[]{:S(2)}) copy-start(bf16[256,3072]{1,0:T(8,128)(2,1)} %copy-done.1) | copy-start | bytes 4718596
  193.5 69.1 %copy-start.4 = (bf16[256,3072]{1,0:T(8,128)(2,1)S(1)}, bf16[256,3072]{1,0:T(8,128)(2,1)}, u32[]{:S(2)}) copy-start(bf16[256,3072]{1,0:T(8,128)(2,1)} %copy-done.3) | copy-start | bytes 4718596
  261.3 50.5 %collective-permute-start.5 = (bf16[256,3072]{1,0:T(8,128)(2,1)}, bf16[256,3072]{1,0:T(8,128)(2,1)S(1)}, u32[]{:S(2)}, u32[]{:S(2)}) collective-permute-start(bf16[256,3072]{1,0:T(8,128)(2,1)} %collective-permute-done.4), channel_id=1, source_target_pairs={{0,4},{4,8},{8,12},{12,16},{16,20},{20,24},{24,28},{28,0},{1,5},{5... | collective-permute-start | bytes 4718600 | tf_op jit(solution)/shard_map/ppermute | solution.py:22
  311.8 32.2 %collective-permute-start.6 = (bf16[256,3072]{1,0:T(8,128)(2,1)S(1)}, bf16[256,3072]{1,0:T(8,128)(2,1)S(1)}, u32[]{:S(2)}, u32[]{:S(2)}) collective-permute-start(bf16[256,3072]{1,0:T(8,128)(2,1)S(1)} %collective-permute-done.5), channel_id=1, source_target_pairs={{0,4},{4,8},{8,12},{12,16},{16,20},{20,24},{24,28},{28,0},{1,5},{5... | collective-permute-start | bytes 4718600 | tf_op jit(solution)/shard_map/ppermute | solution.py:22
  394.8 22.3 %all-to-all-start = ((bf16[4,2,49152]{2,1,0:T(2,128)(2,1)}), bf16[4,2,49152]{2,1,0:T(2,128)(2,1)S(1)}, u32[]{:S(2)}, u32[]{:S(2)}) async-start(bf16[4,2,49152]{2,1,0:T(2,128)(2,1)} %reshape.178), calls=%async_computation | async-start | bytes 1572864 | tf_op jit(solution)/shard_map/all_to_all | solution.py:86
  427.2 2.5 slice-start
  427.8 2.4 slice-start.1
Sparse Core Ops, SparseCore 0:
  131.3 152.6 all-gather.2
  384.9 32.4 all-gather.4
